TPU v7x, 512 devices: a whole 4x8x8 slice. The times are simulated.
512 devices in a mesh: sp: 64 (over z, y), tp: 4 (over x), dp: 2 (over core).
Axes of the slice: x: 4, y: 8, z: 8, core: 2. Of those that a mesh axis runs over, the one named last changes fastest.
Arguments:
- latent: bfloat16 [2, 8192, 2048], P('dp', ('sp', 'tp')), may hold values from -10 to 10
- condition: bfloat16 [2, 2048], P('dp'), may hold values from -6 to 6
- context: bfloat16 [2, 512, 2048], P('dp', 'sp'), may hold values from -6 to 6
- context_source: bfloat16 [2048], replicated, may hold values from -6 to 6
- mod_weight: bfloat16 [3, 2048, 2048], P(None, 'sp', 'tp'), may hold values from -0.125 to 0.125
- norm_gain: bfloat16 [2048], replicated, may hold values from 0.099609375 to 1.8984375
- w_x: bfloat16 [2048, 2048], P('dp', 'tp'), may hold values from -0.125 to 0.125
- w_b: bfloat16 [2048, 512], P('dp', 'tp'), may hold values from -0.125 to 0.125
- w_c: bfloat16 [2048, 512], P('dp', 'tp'), may hold values from -0.125 to 0.125
- w_z: bfloat16 [2048, 2048], P('dp', 'tp'), may hold values from -0.125 to 0.125
- w_dt: bfloat16 [2, 2048, 32], P(None, 'dp', 'tp'), may hold values from -0.125 to 0.125
- conv_x: bfloat16 [3, 2048], P(None, 'tp'), may hold values from -3.5 to 3.5
- conv_b: bfloat16 [3, 512], P(None, 'tp'), may hold values from -3.5 to 3.5
- conv_c: bfloat16 [3, 512], P(None, 'tp'), may hold values from -3.5 to 3.5
- decay_rate: float32 [2, 32], P(None, 'tp'), may hold values from 0 to 1, as said below
- out_gain: bfloat16 [2048], P('tp'), may hold values from 0.099609375 to 1.8984375
- w_out: bfloat16 [2048, 2048], P(('tp', 'dp')), may hold values from -0.125 to 0.125
Outputs:
- update: bfloat16 [2, 8192, 2048], P('dp', ('sp', 'tp'))
Inputs may be any that keep to these rules, and one draw needn't show every extreme that they name: `decay_rate`: positive rates.
All inputs are finite; a program needn't handle non-finite values.
Results may differ from a plain program's by a relative error of at most 0.014.
Values may be sent and summed in bfloat16 or wider, within the bound.
A program may use at most 128 MiB of HBM per device.

v0:
```python
import functools
import jax
import jax.numpy as jnp
from jax import lax
from jax.sharding import Mesh
from jax.sharding import PartitionSpec as P

STATE = 128
BLOCK = 128
SP = ("sp_0", "sp_1")
SP_TP = ("sp_0", "sp_1", "tp")
EPSILON = 1e-06


def over_axes(x, axes):
    return functools.reduce(lax.psum, axes, x)


def laid_out(tiles, dim):
    tiles = jnp.moveaxis(tiles, 0, dim)
    dims = tiles.shape
    return tiles.reshape(*dims[:dim], dims[dim] * dims[dim + 1], *dims[dim + 2 :])


def sent_to_all(x, axis):
    peers = lax.axis_size(axis)
    return lax.all_to_all(jnp.broadcast_to(x[None], (peers, *x.shape)), axis, 0, 0, tiled=True)


def gather_directly(x, axis, dim):
    return laid_out(sent_to_all(x, axis), dim)


def sent_together(arrays, axis, dim, along):
    ends, at = ([], 0)
    for a in arrays[:-1]:
        at += a.shape[along]
        ends.append(at)
    both = jnp.concatenate(arrays, axis=along)
    return tuple(jnp.split(lax.all_gather(both, axis, axis=dim, tiled=True), ends, axis=along))


def with_halo(x, sides, width):
    for axis, dim in sides:
        peers, length = (lax.axis_size(axis), x.shape[dim])
        up = [(i, (i + 1) % peers) for i in range(peers - 1)]
        down = [(j, i) for i, j in up]
        last = lax.slice_in_dim(x, length - width, length, axis=dim)
        leading = lax.slice_in_dim(x, 0, width, axis=dim)
        before = lax.ppermute(last, axis, up)
        after = lax.ppermute(leading, axis, down)
        x = jnp.concatenate([before, x, after], axis=dim)
    return x


def neutral_like(x, identity):
    return jax.tree.map(
        lambda a, e: jnp.broadcast_to(jnp.asarray(e, a.dtype), a.shape), x, identity
    )


def entering_2(x, axes, combine, identity, reverse):
    before = start = neutral_like(x, identity)
    total = x
    for axis in reversed(axes):
        peers, place = (lax.axis_size(axis), lax.axis_index(axis))
        pieces = jax.tree.map(
            lambda part, kind: lax.all_gather(part.astype(kind), axis),
            total,
            (jnp.bfloat16, jnp.bfloat16),
        )
        inside, total = (start, start)
        for k in reversed(range(peers)) if reverse else range(peers):
            passed = k > place if reverse else k < place
            total = combine(
                total, jax.tree.map(lambda part, own: part[k].astype(own.dtype), pieces, x)
            )
            inside = jax.tree.map(lambda new, old: jnp.where(passed, new, old), total, inside)
        before = combine(inside, before)
    return before


def split_up(x, dim, peers):
    before, after = (x.shape[:dim], x.shape[dim + 1 :])
    return jnp.moveaxis(x.reshape(*before, peers, -1, *after), dim, 0)


def sum_at_owner(x, axis, dim):
    peers = lax.axis_size(axis)
    tiles = lax.all_to_all(split_up(x, dim, peers), axis, 0, 0, tiled=True)
    return jnp.sum(tiles.astype(jnp.float32), axis=0)


def rounded(values):
    return lax.optimization_barrier(values.astype(jnp.bfloat16)).astype(jnp.float32)


def modulated(source, gain_vec, shift_vec, scale_vec):
    values = source.astype(jnp.float32)
    normed = values * lax.rsqrt(jnp.mean(values * values, axis=-1, keepdims=True) + EPSILON)
    return (normed * gain_vec.astype(jnp.float32) * (1.0 + scale_vec) + shift_vec).astype(
        jnp.bfloat16
    )


def convolved(padded, weight, total_rows):
    wide_vals = padded.astype(jnp.float32)
    tap_weights = weight.astype(jnp.float32)
    summed = jnp.zeros((total_rows, wide_vals.shape[1]), jnp.float32)
    for offset in range(weight.shape[0]):
        summed = summed + wide_vals[offset : offset + total_rows] * tap_weights[offset]
    return jax.nn.silu(summed).astype(jnp.bfloat16)


def final_state(x_vals, b_vals, step_size, rate_head, groups):
    total_rows, head_count = step_size.shape
    per_group = head_count // groups
    moved_x = rounded(
        x_vals.reshape(total_rows, head_count, -1).astype(jnp.float32) * step_size[:, :, None]
    )
    running = jnp.cumsum(-rate_head * step_size, axis=0)
    weight = jnp.exp(running[-1:] - running)
    scaled = (moved_x * weight[:, :, None]).reshape(total_rows, groups, per_group, -1)
    b_wide = b_vals.reshape(total_rows, groups, -1).astype(jnp.float32)
    ctx_state = jnp.einsum("sgn,sghp->ghpn", b_wide, scaled)
    return (ctx_state, running[-1].reshape(groups, per_group))


def combine_states(earlier, later_part):
    return (
        earlier[0] + later_part[0],
        earlier[1] * jnp.exp(later_part[0])[:, :, None, None] + later_part[1],
    )


def direction_terms(x_vals, b_vals, c_vals, step_size, rate_head, groups):
    total_rows, head_count = step_size.shape
    per_group = head_count // groups
    blocks = total_rows // BLOCK
    moved_x = (
        x_vals.reshape(total_rows, head_count, -1).astype(jnp.float32) * step_size[:, :, None]
    ).astype(jnp.bfloat16)
    head_dim = moved_x.shape[2]
    x_blocks = moved_x.reshape(blocks, BLOCK, groups, per_group, head_dim)
    b_blocks = b_vals.reshape(blocks, BLOCK, groups, -1)
    c_blocks = c_vals.reshape(blocks, BLOCK, groups, -1)
    running = jnp.cumsum((-rate_head * step_size).reshape(blocks, BLOCK, head_count), axis=1)
    across = jnp.swapaxes(running, 1, 2)
    spread = across[:, :, :, None] - across[:, :, None, :]
    lower_part = lax.broadcasted_iota(jnp.int32, (BLOCK, BLOCK), 0) >= lax.broadcasted_iota(
        jnp.int32, (BLOCK, BLOCK), 1
    )
    decay_mask = jnp.where(lower_part, jnp.exp(jnp.minimum(spread, 0.0)), 0.0).reshape(
        blocks, groups, per_group, BLOCK, BLOCK
    )
    scores = jnp.einsum("clgn,csgn->cgls", c_blocks, b_blocks, preferred_element_type=jnp.float32)
    weights = (scores[:, :, None] * decay_mask).astype(jnp.bfloat16)
    inside = jnp.einsum("cghls,csghp->clghp", weights, x_blocks, preferred_element_type=jnp.float32)
    to_end = jnp.exp(running[:, -1:, :] - running).reshape(blocks, BLOCK, groups, per_group, 1)
    x_end = (x_blocks.astype(jnp.float32) * to_end).astype(jnp.bfloat16)
    fresh_state = jnp.einsum(
        "csgn,csghp->cghpn", b_blocks, x_end, preferred_element_type=jnp.float32
    )
    totals = running[:, -1, :].reshape(blocks, groups, per_group)

    def advance(carried_in, inputs):
        return (carried_in * jnp.exp(inputs[1])[:, :, None, None] + inputs[0], carried_in)

    ending, before = lax.scan(
        advance, jnp.zeros(fresh_state.shape[1:], jnp.float32), (fresh_state, totals)
    )
    return (inside, before, ending, totals, running, c_blocks)


def direction_output(terms, incoming):
    inside, before, ending, totals, running, c_blocks = terms
    blocks, length, groups, per_group, head_dim = inside.shape
    offset_sum = jnp.cumsum(totals, axis=0) - totals
    entering = before + jnp.exp(offset_sum)[:, :, :, None, None] * incoming[None]
    carried = jnp.einsum(
        "clgn,cghpn->clghp",
        c_blocks,
        entering.astype(jnp.bfloat16),
        preferred_element_type=jnp.float32,
    )
    growth = jnp.exp(running).reshape(blocks, length, groups, per_group, 1)
    return (inside + growth * carried).reshape(blocks * length, -1)


def shards(
    latent,
    condition,
    context,
    context_source,
    mod_weight,
    norm_gain,
    w_x,
    w_b,
    w_c,
    w_z,
    w_dt,
    conv_x,
    conv_b,
    conv_c,
    decay_rate,
    out_gain,
    w_out,
):
    row_count = mod_weight.shape[1]
    activations = jnp.stack(
        [
            jax.nn.silu(condition[0].astype(jnp.float32)),
            jax.nn.silu(context_source.astype(jnp.float32)),
        ]
    ).astype(jnp.bfloat16)
    own_rows = lax.dynamic_slice_in_dim(activations, lax.axis_index(SP) * row_count, row_count, 1)
    partial_value = jnp.einsum(
        "ar,krc->kac", own_rows, mod_weight, preferred_element_type=jnp.float32
    )
    summed = over_axes(partial_value, SP)
    mod_vectors = gather_directly(summed, "tp", 2)
    full_x, full_b, full_c, full_z, full_fwd, full_bwd, full_out = (
        *sent_together((w_x, w_b, w_c, w_z, w_dt[0], w_dt[1]), "dp", 0, 1),
        lax.all_gather(w_out, "dp", axis=0, tiled=True),
    )
    inner_cols = full_x.shape[1]
    gn_cols = full_b.shape[1]
    head_count = full_fwd.shape[1]
    groups = gn_cols // STATE
    mixed_cols = inner_cols + gn_cols
    reach_rows = conv_x.shape[0] // 2
    rate_fwd = decay_rate[0]
    rate_bwd = decay_rate[1]
    all_weights = jnp.concatenate([full_x, full_b, full_c, full_fwd, full_bwd, full_z], axis=1)
    ctx_weight = jnp.concatenate([full_x, full_b, full_fwd, full_bwd], axis=1)
    taps_all = jnp.concatenate([conv_x, conv_b, conv_c], axis=1)
    ctx_taps = jnp.concatenate([conv_x, conv_b], axis=1)
    ctx_rows = modulated(context[0], norm_gain, mod_vectors[0, 1], mod_vectors[1, 1])
    own_features = jnp.dot(ctx_rows, ctx_weight, preferred_element_type=jnp.float32).astype(
        jnp.bfloat16
    )
    features = gather_directly(own_features, SP, 0)
    total_rows = features.shape[0]
    padded = jnp.pad(features[:, :mixed_cols], ((reach_rows, reach_rows), (0, 0)))
    smoothed = convolved(padded, ctx_taps, total_rows)
    step_size = jax.nn.softplus(features[:, mixed_cols:].astype(jnp.float32))
    ctx_x = smoothed[:, :inner_cols]
    ctx_b = smoothed[:, inner_cols:]
    state_fwd, _ = final_state(ctx_x, ctx_b, step_size[:, :head_count], rate_fwd, groups)
    state_bwd, _ = final_state(
        jnp.flip(ctx_x, 0),
        jnp.flip(ctx_b, 0),
        jnp.flip(step_size[:, head_count:], 0),
        rate_bwd,
        groups,
    )
    latent_rows = modulated(latent[0], norm_gain, mod_vectors[0, 0], mod_vectors[1, 0])
    features = jnp.dot(
        gather_directly(latent_rows, "tp", 0), all_weights, preferred_element_type=jnp.float32
    ).astype(jnp.bfloat16)
    total_rows = features.shape[0]
    padded = with_halo(features[:, : mixed_cols + gn_cols], ((SP, 0),), reach_rows)
    smoothed = convolved(padded, taps_all, total_rows)
    x_vals = smoothed[:, :inner_cols]
    b_vals = smoothed[:, inner_cols:mixed_cols]
    c_vals = smoothed[:, mixed_cols:]
    base_col = mixed_cols + gn_cols
    step_size = jax.nn.softplus(
        features[:, base_col : base_col + 2 * head_count].astype(jnp.float32)
    )
    gate_in = features[:, base_col + 2 * head_count :]
    forward_terms = direction_terms(
        x_vals, b_vals, c_vals, step_size[:, :head_count], rate_fwd, groups
    )
    backward_terms = direction_terms(
        jnp.flip(x_vals, 0),
        jnp.flip(b_vals, 0),
        jnp.flip(c_vals, 0),
        jnp.flip(step_size[:, head_count:], 0),
        rate_bwd,
        groups,
    )
    fwd_total = jnp.sum(forward_terms[3], axis=0)
    bwd_total = jnp.sum(backward_terms[3], axis=0)
    empty = (jnp.zeros_like(fwd_total), jnp.zeros_like(forward_terms[2]))
    prefix_decay, prefix_state = entering_2(
        (fwd_total, forward_terms[2]), SP, combine_states, empty, False
    )
    suffix_decay, suffix_state = entering_2(
        (bwd_total, backward_terms[2]), SP, combine_states, empty, True
    )
    out_fwd = direction_output(
        forward_terms, prefix_state + jnp.exp(prefix_decay)[:, :, None, None] * state_fwd
    )
    out_bwd = jnp.flip(
        direction_output(
            backward_terms, suffix_state + jnp.exp(suffix_decay)[:, :, None, None] * state_bwd
        ),
        0,
    )
    gated = (out_fwd + out_bwd) * jax.nn.silu(gate_in.astype(jnp.float32))
    grouped = gated.reshape(total_rows, groups, -1)
    normed = (
        grouped
        * lax.rsqrt(jnp.mean(grouped * grouped, axis=-1, keepdims=True) + EPSILON)
        * out_gain.reshape(groups, -1).astype(jnp.float32)
    )
    normed_out = normed.reshape(total_rows, -1).astype(jnp.bfloat16)
    mixed = sum_at_owner(
        jnp.dot(normed_out, full_out, preferred_element_type=jnp.float32).astype(jnp.bfloat16),
        "tp",
        0,
    )
    return (mod_vectors[2, 0] * mixed).astype(jnp.bfloat16)[None]


def solution(mesh):
    torus = Mesh(
        mesh.devices.reshape(8, 8, mesh.shape["tp"], mesh.shape["dp"]), ("sp_0", "sp_1", "tp", "dp")
    )
    placed = (
        P("dp", SP_TP, None),
        P("dp", None),
        P("dp", SP, None),
        P(),
        P(None, SP, "tp"),
        P(),
        P("dp", "tp"),
        P("dp", "tp"),
        P("dp", "tp"),
        P("dp", "tp"),
        P(None, "dp", "tp"),
        P(None, "tp"),
        P(None, "tp"),
        P(None, "tp"),
        P(None, "tp"),
        P("tp"),
        P(("tp", "dp"), None),
    )
    return jax.shard_map(
        shards, mesh=torus, in_specs=placed, out_specs=P("dp", SP_TP, None), check_vma=False
    )
```

profile of v0, /device:TPU:1, one launch (start us, length us, event | category | flops | bytes accessed | tf_op | source)
XLA Modules:
  0.0 347.1 jit_solution(8498954441574411239)
XLA Ops:
  7.7 5.4 %concatenate.20 = bf16[1024,1296]{1,0:T(8,128)(2,1)} concatenate(bf16[1024,512]{1,0:T(8,128)(2,1)} %param.23, bf16[1024,128]{1,0:T(8,128)(2,1)} %param.24, bf16[1024,128]{1,0:T(8,128)(2,1)} %param.25, bf16[1024,512]{1,0:T(8,128)(2,1)} %param.26, bf16[1024,8]{1,0:T(8,128)(2,1)S(1)} %copy.97, bf16[1024,8]{1,0:T(8,128)(2,1)S(1)} %copy.98), dimensions={1} | concatenate | bytes 5308416 | tf_op jit(solution)/shard_map/concatenate | solution.py:39
  14.0 29.8 %psum.14 = f32[3,2,512]{2,1,0:T(2,128)S(1)} all-reduce(f32[3,2,512]{2,1,0:T(2,128)S(1)} %convolution_bitcast_fusion.4), channel_id=1, replica_groups=mesh['sp_0'=8,'sp_1'=8,'tp'=4,'dp'=2] {'sp_0'}, use_global_device_ids=true, to_apply=%region_0.1 | all-reduce | flops 3072 | bytes 24576 | tf_op jit(solution)/shard_map/psum | solution.py:16
  43.8 23.1 %psum.15 = f32[3,2,512]{2,1,0:T(2,128)S(1)} all-reduce(f32[3,2,512]{2,1,0:T(2,128)S(1)} %psum.14), channel_id=1, replica_groups=mesh['sp_0'=8,'sp_1'=8,'tp'=4,'dp'=2] {'sp_1'}, use_global_device_ids=true, to_apply=%region_1.2 | all-reduce | flops 3072 | bytes 24576 | tf_op jit(solution)/shard_map/psum | solution.py:16
  67.5 4.0 %all-to-all-start = ((f32[4,3,2,512]{3,2,1,0:T(2,128)}), f32[4,3,2,512]{3,2,1,0:T(2,128)S(1)}, u32[]{:S(2)}, u32[]{:S(2)}) async-start(f32[4,3,2,512]{3,2,1,0:T(2,128)} %broadcast_in_dim.22), calls=%async_computation | async-start | bytes 98304 | tf_op jit(solution)/shard_map/all_to_all | solution.py:27
  71.7 4.2 %all-to-all-done = f32[4,3,2,512]{3,2,1,0:T(2,128)S(1)} async-done(((f32[4,3,2,512]{3,2,1,0:T(2,128)}), f32[4,3,2,512]{3,2,1,0:T(2,128)S(1)}, u32[]{:S(2)}, u32[]{:S(2)}) %all-to-all-start) | async-done | bytes 49184 | tf_op jit(solution)/shard_map/all_to_all | solution.py:27
  77.5 4.1 %all-to-all-start.1 = ((bf16[4,32,2048]{2,1,0:T(8,128)(2,1)}), bf16[4,32,2048]{2,1,0:T(8,128)(2,1)}, u32[]{:S(2)}, u32[]{:S(2)}) async-start(bf16[4,32,2048]{2,1,0:T(8,128)(2,1)} %broadcast_in_dim.24), calls=%async_computation.1 | async-start | bytes 1048576 | tf_op jit(solution)/shard_map/all_to_all | solution.py:27
  83.8 3.1 split.20
  88.9 9.4 %concatenate.21 = bf16[2048,1296]{1,0:T(8,128)(2,1)} concatenate(bf16[2048,768]{1,0:T(8,128)(2,1)S(1)} %split.18, bf16[2048,16]{1,0:T(8,128)(2,1)} %split.19, bf16[2048,512]{1,0:T(8,128)(2,1)} %split.20), dimensions={1} | concatenate | bytes 10616832 | tf_op jit(solution)/shard_map/concatenate | solution.py:234
  98.3 5.1 %convolution_convert_fusion.1 = bf16[128,1296]{0,1:T(8,128)(2,1)S(1)} fusion(bf16[128,2048]{1,0:T(8,128)(2,1)} %bitcast.7, bf16[2048,1296]{1,0:T(8,128)(2,1)} %concatenate.21), kind=kOutput, calls=%fused_computation.5 | convolution fusion | flops 679643136 | bytes 6164480 | tf_op jit(solution)/shard_map/dot_general | solution.py:258
  109.1 3.8 %collective-permute-done.1 = bf16[1,768]{0,1:T(8,128)(2,1)S(1)} collective-permute-done((bf16[1,768]{0,1:T(8,128)(2,1)S(1)}, bf16[1,768]{0,1:T(8,128)(2,1)S(1)}, u32[]{:S(2)}, u32[]{:S(2)}) %collective-permute-start.1) | collective-permute-done | bytes 1568 | tf_op jit(solution)/shard_map/ppermute | solution.py:51
  118.5 13.1 %all_gather.48 = bf16[8,1,8]{2,1,0:T(2,128)(2,1)S(1)} all-gather(bf16[1,1,8]{2,1,0:T(2,128)(2,1)S(1)} %slice.999), channel_id=1, replica_groups=mesh['sp_0'=8,'sp_1'=8,'tp'=4,'dp'=2] {'sp_1'}, dimensions={0}, use_global_device_ids=true | all-gather | bytes 144 | tf_op jit(solution)/shard_map/all_gather | solution.py:68
  131.7 35.6 %all-gather.19.cloned.1.call-done = bf16[64,64,128]{2,1,0:T(8,128)(2,1)} async-done(((bf16[8,64,128]{2,1,0:T(8,128)(2,1)}), bf16[64,64,128]{2,1,0:T(8,128)(2,1)}) %all-gather.19.cloned.1.call-update) | async-done | bytes 1048592 | tf_op jit(solution)/shard_map/all_gather | solution.py:68
  169.6 11.2 %all_gather.43 = bf16[8,1,8]{2,1,0:T(2,128)(2,1)S(1)} all-gather(bf16[1,1,8]{2,1,0:T(2,128)(2,1)S(1)} %slice.1000), channel_id=1, replica_groups=mesh['sp_0'=8,'sp_1'=8,'tp'=4,'dp'=2] {'sp_1'}, dimensions={0}, use_global_device_ids=true | all-gather | bytes 144 | tf_op jit(solution)/shard_map/all_gather | solution.py:68
  180.9 28.2 %all-gather.17.cloned.1.call-done = bf16[64,64,128]{2,1,0:T(8,128)(2,1)} async-done(((bf16[8,64,128]{2,1,0:T(8,128)(2,1)}), bf16[64,64,128]{2,1,0:T(8,128)(2,1)}) %all-gather.17.cloned.1.call-update) | async-done | bytes 1048592 | tf_op jit(solution)/shard_map/all_gather | solution.py:68
  213.4 13.5 %all_gather.49 = bf16[8,1,8]{2,1,0:T(2,128)(2,1)S(1)} all-gather(bf16[1,1,8]{2,1,0:T(2,128)(2,1)S(1)} %get-tuple-element.103), channel_id=1, replica_groups=mesh['sp_0'=8,'sp_1'=8,'tp'=4,'dp'=2] {'sp_0'}, dimensions={0}, use_global_device_ids=true | all-gather | bytes 144 | tf_op jit(solution)/shard_map/all_gather | solution.py:68
  227.6 10.5 %all_gather.44 = bf16[8,1,8]{2,1,0:T(2,128)(2,1)S(1)} all-gather(bf16[1,1,8]{2,1,0:T(2,128)(2,1)S(1)} %get-tuple-element.83), channel_id=1, replica_groups=mesh['sp_0'=8,'sp_1'=8,'tp'=4,'dp'=2] {'sp_0'}, dimensions={0}, use_global_device_ids=true | all-gather | bytes 144 | tf_op jit(solution)/shard_map/all_gather | solution.py:68
  242.2 8.2 %all-to-all-start.2 = ((bf16[64,8,656]{2,1,0:T(8,128)(2,1)}), bf16[64,8,656]{2,1,0:T(8,128)(2,1)S(1)}, u32[]{:S(2)}, u32[]{:S(2)}) async-start(bf16[64,8,656]{2,1,0:T(8,128)(2,1)} %broadcast_in_dim.26), calls=%async_computation.2 | async-start | bytes 1572864 | tf_op jit(solution)/shard_map/all_to_all | solution.py:27
  255.4 11.4 %all-to-all-done.2 = bf16[64,8,656]{2,1,0:T(8,128)(2,1)S(1)} async-done(((bf16[64,8,656]{2,1,0:T(8,128)(2,1)}), bf16[64,8,656]{2,1,0:T(8,128)(2,1)S(1)}, u32[]{:S(2)}, u32[]{:S(2)}) %all-to-all-start.2) | async-done | bytes 671776 | tf_op jit(solution)/shard_map/all_to_all | solution.py:27
  277.3 6.3 %rev.35 = bf16[512,512]{1,0:T(8,128)(2,1)S(1)} reverse(bf16[512,512]{1,0:T(8,128)(2,1)} %get-tuple-element.48), dimensions={0} | reverse | bytes 1048576 | tf_op jit(solution)/shard_map/jit(_flip)/rev | solution.py:251
  284.7 3.3 fusion.13
  289.7 10.8 %all-gather.11.cloned.1.call-done = bf16[8,1,8,64,128]{4,3,2,1,0:T(8,128)(2,1)} async-done(((bf16[1,1,8,64,128]{4,3,2,1,0:T(8,128)(2,1)}), bf16[8,1,8,64,128]{4,3,2,1,0:T(8,128)(2,1)}) %all-gather.11.cloned.1.call-update) | async-done | bytes 1048592 | tf_op jit(solution)/shard_map/all_gather | solution.py:68
  300.8 2.6 fusion.12
  303.9 21.7 %all-gather.15.cloned.1.call-done = bf16[512,2048]{1,0:T(8,128)(2,1)} async-done(((bf16[256,2048]{1,0:T(8,128)(2,1)}), bf16[512,2048]{1,0:T(8,128)(2,1)}) %all-gather.15.cloned.1.call-update) | async-done | bytes 2097168 | tf_op jit(solution)/shard_map/all_gather | solution.py:224
  327.7 11.9 %all_to_all.20 = bf16[4,32,2048]{2,1,0:T(8,128)(2,1)S(1)} all-to-all(bf16[4,32,2048]{2,1,0:T(8,128)(2,1)S(1)} %bitcast.494), channel_id=1, replica_groups=mesh['sp_0'=8,'sp_1'=8,'tp'=4,'dp'=2] {'tp'}, dimensions={0} | all-to-all | bytes 1048576 | tf_op jit(solution)/shard_map/all_to_all | solution.py:90
  (295 shorter events, 52.0 us)
Async XLA Ops:
  6.5 75.3 %all-gather.9.cloned.1.call-start = ((), (), s32[]{:S(2)}) async-start(), calls=%async_computation.4 | async-start | bytes 8650752 | tf_op jit(solution)/shard_map/all_gather | solution.py:40
  13.1 58.5 %copy-start.3 = (bf16[1,32,2048]{2,1,0:T(8,128)(2,1)S(1)}, bf16[1,32,2048]{2,1,0:T(8,128)(2,1)}, u32[]{:S(2)}) copy-start(bf16[1,32,2048]{2,1,0:T(8,128)(2,1)} %param.17) | copy-start | bytes 393220
  13.1 58.6 %copy-start.25 = (bf16[2048]{0:T(1024)(128)(2,1)S(1)}, bf16[2048]{0:T(1024)(128)(2,1)}, u32[]{:S(2)}) copy-start(bf16[2048]{0:T(1024)(128)(2,1)} %param.22) | copy-start | bytes 12292
  13.1 68.6 %copy-start.15 = (bf16[3,512]{1,0:T(4,128)(2,1)S(1)}, bf16[3,512]{1,0:T(4,128)(2,1)}, u32[]{:S(2)}) copy-start(bf16[3,512]{1,0:T(4,128)(2,1)} %param.28) | copy-start | bytes 9220
  13.1 68.6 %copy-start.30 = (bf16[3,128]{1,0:T(4,128)(2,1)S(1)}, bf16[3,128]{1,0:T(4,128)(2,1)}, u32[]{:S(2)}) copy-start(bf16[3,128]{1,0:T(4,128)(2,1)} %param.29) | copy-start | bytes 2308
  13.1 68.6 %copy-start.66 = (bf16[3,128]{1,0:T(4,128)(2,1)S(1)}, bf16[3,128]{1,0:T(4,128)(2,1)}, u32[]{:S(2)}) copy-start(bf16[3,128]{1,0:T(4,128)(2,1)} %param.30) | copy-start | bytes 2308
  13.1 68.7 %copy-start.68 = (f32[2,8]{1,0:T(2,128)S(1)}, f32[2,8]{1,0:T(2,128)}, u32[]{:S(2)}) copy-start(f32[2,8]{1,0:T(2,128)} %param.31) | copy-start | bytes 196
  67.5 8.4 %all-to-all-start = ((f32[4,3,2,512]{3,2,1,0:T(2,128)}), f32[4,3,2,512]{3,2,1,0:T(2,128)S(1)}, u32[]{:S(2)}, u32[]{:S(2)}) async-start(f32[4,3,2,512]{3,2,1,0:T(2,128)} %broadcast_in_dim.22), calls=%async_computation | async-start | bytes 98304 | tf_op jit(solution)/shard_map/all_to_all | solution.py:27
  77.5 20.8 %all-to-all-start.1 = ((bf16[4,32,2048]{2,1,0:T(8,128)(2,1)}), bf16[4,32,2048]{2,1,0:T(8,128)(2,1)}, u32[]{:S(2)}, u32[]{:S(2)}) async-start(bf16[4,32,2048]{2,1,0:T(8,128)(2,1)} %broadcast_in_dim.24), calls=%async_computation.1 | async-start | bytes 1048576 | tf_op jit(solution)/shard_map/all_to_all | solution.py:27
  81.7 85.5 %all-gather.19.cloned.1.call-start = ((), (), s32[]{:S(2)}) async-start(), calls=%async_computation.9 | async-start | bytes 1179648 | tf_op jit(solution)/shard_map/all_gather | solution.py:68
  104.8 4.3 %collective-permute-start = (bf16[1,768]{0,1:T(8,128)(2,1)S(1)}, bf16[1,768]{0,1:T(8,128)(2,1)S(1)}, u32[]{:S(2)}, u32[]{:S(2)}) collective-permute-start(bf16[1,768]{0,1:T(8,128)(2,1)S(1)} %get-tuple-element.49), channel_id=1, source_target_pairs={{0,8},{8,16},{16,24},{24,32},{32,40},{40,48},{48,56},{56,64},{64,7... | collective-permute-start | bytes 4616 | tf_op jit(solution)/shard_map/ppermute | solution.py:50
  106.5 6.4 %collective-permute-start.1 = (bf16[1,768]{0,1:T(8,128)(2,1)S(1)}, bf16[1,768]{0,1:T(8,128)(2,1)S(1)}, u32[]{:S(2)}, u32[]{:S(2)}) collective-permute-start(bf16[1,768]{0,1:T(8,128)(2,1)S(1)} %get-tuple-element.50), channel_id=1, source_target_pairs={{8,0},{16,8},{24,16},{32,24},{40,32},{48,40},{56,48},{64,56},{72,6... | collective-permute-start | bytes 4616 | tf_op jit(solution)/shard_map/ppermute | solution.py:51
  115.9 93.1 %all-gather.17.cloned.1.call-start = ((), (), s32[]{:S(2)}) async-start(), calls=%async_computation.8 | async-start | bytes 1179648 | tf_op jit(solution)/shard_map/all_gather | solution.py:68
  117.5 94.5 %copy-start.16 = (bf16[3,512]{1,0:T(4,128)(2,1)S(1)}, bf16[3,512]{1,0:T(4,128)(2,1)}, u32[]{:S(2)}) copy-start(bf16[3,512]{1,0:T(4,128)(2,1)} %param.28) | copy-start | bytes 9220
  117.6 94.5 %copy-start.31 = (bf16[3,128]{1,0:T(4,128)(2,1)S(1)}, bf16[3,128]{1,0:T(4,128)(2,1)}, u32[]{:S(2)}) copy-start(bf16[3,128]{1,0:T(4,128)(2,1)} %param.29) | copy-start | bytes 2308
  117.6 95.1 %copy-start.11 = (bf16[1,8,2048]{2,1,0:T(8,128)(2,1)S(1)}, bf16[1,8,2048]{2,1,0:T(8,128)(2,1)}, u32[]{:S(2)}) copy-start(bf16[1,8,2048]{2,1,0:T(8,128)(2,1)} %param.19) | copy-start | bytes 98308
  117.6 95.2 %copy-start.67 = (bf16[512]{0:T(512)(128)(2,1)S(1)}, bf16[512]{0:T(512)(128)(2,1)}, u32[]{:S(2)}) copy-start(bf16[512]{0:T(512)(128)(2,1)} %param.32) | copy-start | bytes 3076
  118.5 165.9 %all-gather.13.cloned.1.call-start = ((), (), s32[]{:S(2)}) async-start(), calls=%async_computation.6 | async-start | bytes 1179648 | tf_op jit(solution)/shard_map/all_gather | solution.py:68
  169.5 131.0 %all-gather.11.cloned.1.call-start = ((), (), s32[]{:S(2)}) async-start(), calls=%async_computation.5 | async-start | bytes 1179648 | tf_op jit(solution)/shard_map/all_gather | solution.py:68
  180.8 57.9 %copy-start.37 = (f32[8]{0:T(128)}, f32[8]{0:T(128)S(1)}, u32[]{:S(2)}) copy-start(f32[8]{0:T(128)S(1)} %get-tuple-element.86) | copy-start | bytes 100
  180.8 57.9 %copy-start.39 = (f32[8]{0:T(128)}, f32[8]{0:T(128)S(1)}, u32[]{:S(2)}) copy-start(f32[8]{0:T(128)S(1)} %get-tuple-element.87) | copy-start | bytes 100
  180.9 57.9 %copy-start.41 = (f32[8]{0:T(128)}, f32[8]{0:T(128)S(1)}, u32[]{:S(2)}) copy-start(f32[8]{0:T(128)S(1)} %get-tuple-element.88) | copy-start | bytes 100
  211.4 114.2 %all-gather.15.cloned.1.call-start = ((), (), s32[]{:S(2)}) async-start(), calls=%async_computation.7 | async-start | bytes 3145728 | tf_op jit(solution)/shard_map/all_gather | solution.py:224
  242.2 24.7 %all-to-all-start.2 = ((bf16[64,8,656]{2,1,0:T(8,128)(2,1)}), bf16[64,8,656]{2,1,0:T(8,128)(2,1)S(1)}, u32[]{:S(2)}, u32[]{:S(2)}) async-start(bf16[64,8,656]{2,1,0:T(8,128)(2,1)} %broadcast_in_dim.26), calls=%async_computation.2 | async-start | bytes 1572864 | tf_op jit(solution)/shard_map/all_to_all | solution.py:27
  (71 other events, 1120.1 us)
Sparse Core Ops, SparseCore 0:
  13.3 31.0 all-gather.8
  116.1 51.1 all-gather.18
  169.3 39.7 all-gather.16
  211.0 41.0 all-gather.12
  254.0 46.4 all-gather.10
  302.5 22.9 all-gather.14
where the time goes:
time: 349 us; the launch traced here: 347 us
  waiting for transfers between devices  117 us (34%)
  blocking collectives  113 us (32%)
  local copies, waits for them, and re-layouts  40.7 us (12%)
  other arithmetic  23 us (7%)
  starting transfers between devices  19.6 us (6%)
  matrix products  18.9 us (5%)
  between operations  15 us (4%)
    all_gather x4, waiting for transfers between devices, entering_2(): lax.all_gather(part.astype(kind), axis)  74.5 us
    psum x2, blocking collectives, over_axes(): return functools.reduce(lax.psum, axes, x)  52.9 us
    all_gather x4, blocking collectives, entering_2(): lax.all_gather(part.astype(kind), axis)  48.2 us
    all_gather x1, waiting for transfers between devices, shards(): lax.all_gather(w_out, 'dp', axis=0, tiled=True)  21.7 us
    all_to_all x3, starting transfers between devices, sent_to_all(): lax.all_to_all(jnp.broadcast_to(x[None], (peers, *x.shape)), axis, 0, 0,...  16.4 us
    all_to_all x3, waiting for transfers between devices, sent_to_all(): lax.all_to_all(jnp.broadcast_to(x[None], (peers, *x.shape)), axis, 0, 0,...  15.7 us
    all_to_all x1, blocking collectives, sum_at_owner(): tiles = lax.all_to_all(split_up(x, dim, peers), axis, 0, 0, tiled=True)  11.9 us
    concatenate x1, local copies, waits for them, and re-layouts, shards(): jnp.concatenate([full_x, full_b, full_c, full_fwd, full_bwd, full_z], axi...  9.42 us
  transfers between devices with their start and end apart: 11, of which 8 were waited for; matrix products, arithmetic and copies ran while one was open for 18% of the time, Pallas kernels for 0%

commit v1 on v0

--- a/solution.py
+++ b/solution.py
@@ -221,7 +221,9 @@
     mod_vectors = gather_directly(summed, "tp", 2)
     full_x, full_b, full_c, full_z, full_fwd, full_bwd, full_out = (
         *sent_together((w_x, w_b, w_c, w_z, w_dt[0], w_dt[1]), "dp", 0, 1),
-        lax.all_gather(w_out, "dp", axis=0, tiled=True),
+        jnp.concatenate(
+            lax.all_to_all(jnp.stack([w_out] * lax.axis_size("dp")), "dp", 0, 0), axis=0
+        ),
     )
     inner_cols = full_x.shape[1]
     gn_cols = full_b.shape[1]

time: 349 us -> 360 us (1.032)
  the two profiles are of different devices: /device:TPU:1 before, /device:TPU:8 now
where the time goes in v1:
time: 360 us; the launch traced here: 358 us
  blocking collectives  147 us (41%)
  waiting for transfers between devices  75.5 us (21%)
  local copies, waits for them, and re-layouts  46 us (13%)
  starting transfers between devices  28.9 us (8%)
  other arithmetic  27.3 us (8%)
  matrix products  19.5 us (5%)
  between operations  13.9 us (4%)
    all_gather x4, blocking collectives, entering_2(): lax.all_gather(part.astype(kind), axis)  70.7 us
    all_gather x4, waiting for transfers between devices, entering_2(): lax.all_gather(part.astype(kind), axis)  66.2 us
    psum x2, blocking collectives, over_axes(): return functools.reduce(lax.psum, axes, x)  64.3 us
    all_to_all x3, starting transfers between devices, sent_to_all(): lax.all_to_all(jnp.broadcast_to(x[None], (peers, *x.shape)), axis, 0, 0,...  18.9 us
    all_to_all x1, blocking collectives, sum_at_owner(): tiles = lax.all_to_all(split_up(x, dim, peers), axis, 0, 0, tiled=True)  12.1 us
    concatenate x1, local copies, waits for them, and re-layouts, shards(): jnp.concatenate([full_x, full_b, full_c, full_fwd, full_bwd, full_z], axi...  9.42 us
    split x5, local copies, waits for them, and re-layouts, sent_together(): jnp.split(lax.all_gather(both, axis, axis=dim, tiled=True), ends, axis=al...  8.75 us
    rev x1, local copies, waits for them, and re-layouts, shards(): jnp.flip(ctx_x, 0)  8.31 us
  transfers between devices with their start and end apart: 11, of which 5 were waited for; matrix products, arithmetic and copies ran while one was open for 20% of the time, Pallas kernels for 0%

profile of v1, /device:TPU:8, one launch (start us, length us, event | category | flops | bytes accessed | tf_op | source)
XLA Modules:
  0.0 358.2 jit_solution(13981238978804822432)
XLA Ops:
  7.7 5.4 %concatenate.20 = bf16[1024,1296]{1,0:T(8,128)(2,1)} concatenate(bf16[1024,512]{1,0:T(8,128)(2,1)} %param.23, bf16[1024,128]{1,0:T(8,128)(2,1)} %param.24, bf16[1024,128]{1,0:T(8,128)(2,1)} %param.25, bf16[1024,512]{1,0:T(8,128)(2,1)} %param.26, bf16[1024,8]{1,0:T(8,128)(2,1)S(1)} %copy.97, bf16[1024,8]{1,0:T(8,128)(2,1)S(1)} %copy.98), dimensions={1} | concatenate | bytes 5308416 | tf_op jit(solution)/shard_map/concatenate | solution.py:39
  14.0 35.9 %psum.14 = f32[3,2,512]{2,1,0:T(2,128)S(1)} all-reduce(f32[3,2,512]{2,1,0:T(2,128)S(1)} %convolution_bitcast_fusion.4), channel_id=1, replica_groups=mesh['sp_0'=8,'sp_1'=8,'tp'=4,'dp'=2] {'sp_0'}, use_global_device_ids=true, to_apply=%region_0.1 | all-reduce | flops 3072 | bytes 24576 | tf_op jit(solution)/shard_map/psum | solution.py:16
  49.9 28.4 %psum.15 = f32[3,2,512]{2,1,0:T(2,128)S(1)} all-reduce(f32[3,2,512]{2,1,0:T(2,128)S(1)} %psum.14), channel_id=1, replica_groups=mesh['sp_0'=8,'sp_1'=8,'tp'=4,'dp'=2] {'sp_1'}, use_global_device_ids=true, to_apply=%region_1.2 | all-reduce | flops 3072 | bytes 24576 | tf_op jit(solution)/shard_map/psum | solution.py:16
  79.0 4.3 %all-to-all-start = ((f32[4,3,2,512]{3,2,1,0:T(2,128)}), f32[4,3,2,512]{3,2,1,0:T(2,128)S(1)}, u32[]{:S(2)}, u32[]{:S(2)}) async-start(f32[4,3,2,512]{3,2,1,0:T(2,128)} %broadcast_in_dim.22), calls=%async_computation | async-start | bytes 98304 | tf_op jit(solution)/shard_map/all_to_all | solution.py:27
  83.7 5.1 %all-to-all-done = f32[4,3,2,512]{3,2,1,0:T(2,128)S(1)} async-done(((f32[4,3,2,512]{3,2,1,0:T(2,128)}), f32[4,3,2,512]{3,2,1,0:T(2,128)S(1)}, u32[]{:S(2)}, u32[]{:S(2)}) %all-to-all-start) | async-done | bytes 49184 | tf_op jit(solution)/shard_map/all_to_all | solution.py:27
  89.8 4.1 %all-to-all-start.1 = ((bf16[4,32,2048]{2,1,0:T(8,128)(2,1)}), bf16[4,32,2048]{2,1,0:T(8,128)(2,1)}, u32[]{:S(2)}, u32[]{:S(2)}) async-start(bf16[4,32,2048]{2,1,0:T(8,128)(2,1)} %broadcast_in_dim.24), calls=%async_computation.1 | async-start | bytes 1048576 | tf_op jit(solution)/shard_map/all_to_all | solution.py:27
  98.0 3.1 split.20
  103.2 9.4 %concatenate.21 = bf16[2048,1296]{1,0:T(8,128)(2,1)} concatenate(bf16[2048,768]{1,0:T(8,128)(2,1)S(1)} %split.18, bf16[2048,16]{1,0:T(8,128)(2,1)} %split.19, bf16[2048,512]{1,0:T(8,128)(2,1)} %split.20), dimensions={1} | concatenate | bytes 10616832 | tf_op jit(solution)/shard_map/concatenate | solution.py:236
  112.6 5.1 %convolution_convert_fusion.1 = bf16[128,1296]{0,1:T(8,128)(2,1)S(1)} fusion(bf16[128,2048]{1,0:T(8,128)(2,1)} %bitcast.7, bf16[2048,1296]{1,0:T(8,128)(2,1)} %concatenate.21), kind=kOutput, calls=%fused_computation.5 | convolution fusion | flops 679643136 | bytes 6164480 | tf_op jit(solution)/shard_map/dot_general | solution.py:260
  119.1 3.1 collective-permute-start
  122.2 2.7 collective-permute-start.1
  126.6 3.1 collective-permute-done.1
  139.0 10.5 %all-to-all-start.2 = ((bf16[64,8,656]{2,1,0:T(8,128)(2,1)}), bf16[64,8,656]{2,1,0:T(8,128)(2,1)S(1)}, u32[]{:S(2)}, u32[]{:S(2)}) async-start(bf16[64,8,656]{2,1,0:T(8,128)(2,1)} %broadcast_in_dim.26), calls=%async_computation.2 | async-start | bytes 1572864 | tf_op jit(solution)/shard_map/all_to_all | solution.py:27
  149.6 24.4 %all_gather.45 = bf16[8,1,8]{2,1,0:T(2,128)(2,1)S(1)} all-gather(bf16[1,1,8]{2,1,0:T(2,128)(2,1)S(1)} %slice.999), channel_id=1, replica_groups=mesh['sp_0'=8,'sp_1'=8,'tp'=4,'dp'=2] {'sp_1'}, dimensions={0}, use_global_device_ids=true | all-gather | bytes 144 | tf_op jit(solution)/shard_map/all_gather | solution.py:68
  174.0 17.4 %all_gather.46 = bf16[8,1,8]{2,1,0:T(2,128)(2,1)S(1)} all-gather(bf16[1,1,8]{2,1,0:T(2,128)(2,1)S(1)} %get-tuple-element.103), channel_id=1, replica_groups=mesh['sp_0'=8,'sp_1'=8,'tp'=4,'dp'=2] {'sp_0'}, dimensions={0}, use_global_device_ids=true | all-gather | bytes 144 | tf_op jit(solution)/shard_map/all_gather | solution.py:68
  191.5 14.7 %all_gather.40 = bf16[8,1,8]{2,1,0:T(2,128)(2,1)S(1)} all-gather(bf16[1,1,8]{2,1,0:T(2,128)(2,1)S(1)} %slice.1000), channel_id=1, replica_groups=mesh['sp_0'=8,'sp_1'=8,'tp'=4,'dp'=2] {'sp_1'}, dimensions={0}, use_global_device_ids=true | all-gather | bytes 144 | tf_op jit(solution)/shard_map/all_gather | solution.py:68
  210.0 14.2 %all_gather.41 = bf16[8,1,8]{2,1,0:T(2,128)(2,1)S(1)} all-gather(bf16[1,1,8]{2,1,0:T(2,128)(2,1)S(1)} %get-tuple-element.83), channel_id=1, replica_groups=mesh['sp_0'=8,'sp_1'=8,'tp'=4,'dp'=2] {'sp_0'}, dimensions={0}, use_global_device_ids=true | all-gather | bytes 144 | tf_op jit(solution)/shard_map/all_gather | solution.py:68
  228.3 3.8 %all-to-all-start.3 = ((bf16[2,256,2048]{2,1,0:T(8,128)(2,1)}), bf16[2,256,2048]{2,1,0:T(8,128)(2,1)S(1)}, u32[]{:S(2)}, u32[]{:S(2)}) async-start(bf16[2,256,2048]{2,1,0:T(8,128)(2,1)} %pad_maximum_fusion), calls=%async_computation.3 | async-start | bytes 4194304 | tf_op jit(solution)/shard_map/all_to_all | solution.py:225
  246.7 8.3 %rev.35 = bf16[512,512]{1,0:T(8,128)(2,1)} reverse(bf16[512,512]{1,0:T(8,128)(2,1)} %get-tuple-element.48), dimensions={0} | reverse | bytes 1048576 | tf_op jit(solution)/shard_map/jit(_flip)/rev | solution.py:253
  260.8 29.6 %all-gather.12.cloned.1.call-done = bf16[8,1,8,64,128]{4,3,2,1,0:T(8,128)(2,1)} async-done(((bf16[1,1,8,64,128]{4,3,2,1,0:T(8,128)(2,1)}), bf16[8,1,8,64,128]{4,3,2,1,0:T(8,128)(2,1)}) %all-gather.12.cloned.1.call-update) | async-done | bytes 1048592 | tf_op jit(solution)/shard_map/all_gather | solution.py:68
  290.5 3.7 %fusion.13 = f32[1,128,1,8,64]{1,4,3,2,0:T(8,128)} fusion(bf16[512,8,64]{0,2,1:T(8,128)(2,1)} %multiply_convert_fusion.1, f32[512,8]{0,1:T(8,128)S(1)} %subtract_exponential_fusion, bf16[8,1,8,64,128]{4,3,2,1,0:T(8,128)(2,1)} %all-gather.12.cloned.1.call-done, bf16[512,128]{1,0:T(8,128)(2,1)} %rev.37, f32[8]{0:T(128)} %get-tuple-element.95, ...), kind=kOutput, calls=%fused_computation.28 | convolution fusion | flops 88932352 | bytes 3068528 | tf_op jit(solution)/shard_map/clgn,cghpn->clghp/dot_general | solution.py:180
  295.8 36.5 %all-gather.10.cloned.1.call-done = bf16[8,1,8,64,128]{4,3,2,1,0:T(8,128)(2,1)} async-done(((bf16[1,1,8,64,128]{4,3,2,1,0:T(8,128)(2,1)}), bf16[8,1,8,64,128]{4,3,2,1,0:T(8,128)(2,1)}) %all-gather.10.cloned.1.call-update) | async-done | bytes 1048592 | tf_op jit(solution)/shard_map/all_gather | solution.py:68
  332.4 3.4 fusion.12
  338.7 12.1 %all_to_all.25 = bf16[4,32,2048]{2,1,0:T(8,128)(2,1)S(1)} all-to-all(bf16[4,32,2048]{2,1,0:T(8,128)(2,1)S(1)} %bitcast.497), channel_id=1, replica_groups=mesh['sp_0'=8,'sp_1'=8,'tp'=4,'dp'=2] {'tp'}, dimensions={0} | all-to-all | bytes 1048576 | tf_op jit(solution)/shard_map/all_to_all | solution.py:90
  (217 shorter events, 55.9 us)
Async XLA Ops:
  6.5 89.6 %all-gather.8.cloned.1.call-start = ((), (), s32[]{:S(2)}) async-start(), calls=%async_computation.5 | async-start | bytes 8650752 | tf_op jit(solution)/shard_map/all_gather | solution.py:40
  13.1 70.2 %copy-start.6 = (bf16[1,32,2048]{2,1,0:T(8,128)(2,1)S(1)}, bf16[1,32,2048]{2,1,0:T(8,128)(2,1)}, u32[]{:S(2)}) copy-start(bf16[1,32,2048]{2,1,0:T(8,128)(2,1)} %param.17) | copy-start | bytes 393220
  13.1 70.3 %copy-start.41 = (f32[2,8]{1,0:T(2,128)S(1)}, f32[2,8]{1,0:T(2,128)}, u32[]{:S(2)}) copy-start(f32[2,8]{1,0:T(2,128)} %param.31) | copy-start | bytes 196
  13.1 70.4 %copy-start.12 = (bf16[1,8,2048]{2,1,0:T(8,128)(2,1)S(1)}, bf16[1,8,2048]{2,1,0:T(8,128)(2,1)}, u32[]{:S(2)}) copy-start(bf16[1,8,2048]{2,1,0:T(8,128)(2,1)} %param.19) | copy-start | bytes 98308
  13.1 70.5 %copy-start.23 = (bf16[2048]{0:T(1024)(128)(2,1)S(1)}, bf16[2048]{0:T(1024)(128)(2,1)}, u32[]{:S(2)}) copy-start(bf16[2048]{0:T(1024)(128)(2,1)} %param.22) | copy-start | bytes 12292
  13.1 70.5 %copy-start.14 = (bf16[3,512]{1,0:T(4,128)(2,1)S(1)}, bf16[3,512]{1,0:T(4,128)(2,1)}, u32[]{:S(2)}) copy-start(bf16[3,512]{1,0:T(4,128)(2,1)} %param.28) | copy-start | bytes 9220
  13.1 70.5 %copy-start.26 = (bf16[3,128]{1,0:T(4,128)(2,1)S(1)}, bf16[3,128]{1,0:T(4,128)(2,1)}, u32[]{:S(2)}) copy-start(bf16[3,128]{1,0:T(4,128)(2,1)} %param.29) | copy-start | bytes 2308
  13.1 70.5 %copy-start.39 = (bf16[3,128]{1,0:T(4,128)(2,1)S(1)}, bf16[3,128]{1,0:T(4,128)(2,1)}, u32[]{:S(2)}) copy-start(bf16[3,128]{1,0:T(4,128)(2,1)} %param.30) | copy-start | bytes 2308
  13.2 81.4 %copy-start.4 = (bf16[256,2048]{1,0:T(8,128)(2,1)S(1)}, bf16[256,2048]{1,0:T(8,128)(2,1)}, u32[]{:S(2)}) copy-start(bf16[256,2048]{1,0:T(8,128)(2,1)} %param.33) | copy-start | bytes 3145732
  79.0 9.8 %all-to-all-start = ((f32[4,3,2,512]{3,2,1,0:T(2,128)}), f32[4,3,2,512]{3,2,1,0:T(2,128)S(1)}, u32[]{:S(2)}, u32[]{:S(2)}) async-start(f32[4,3,2,512]{3,2,1,0:T(2,128)} %broadcast_in_dim.22), calls=%async_computation | async-start | bytes 98304 | tf_op jit(solution)/shard_map/all_to_all | solution.py:27
  89.8 22.8 %all-to-all-start.1 = ((bf16[4,32,2048]{2,1,0:T(8,128)(2,1)}), bf16[4,32,2048]{2,1,0:T(8,128)(2,1)}, u32[]{:S(2)}, u32[]{:S(2)}) async-start(bf16[4,32,2048]{2,1,0:T(8,128)(2,1)} %broadcast_in_dim.24), calls=%async_computation.1 | async-start | bytes 1048576 | tf_op jit(solution)/shard_map/all_to_all | solution.py:27
  94.0 138.3 %all-gather.16.cloned.1.call-start = ((), (), s32[]{:S(2)}) async-start(), calls=%async_computation.9 | async-start | bytes 1179648 | tf_op jit(solution)/shard_map/all_gather | solution.py:68
  119.1 7.6 %collective-permute-start = (bf16[1,768]{0,1:T(8,128)(2,1)S(1)}, bf16[1,768]{0,1:T(8,128)(2,1)S(1)}, u32[]{:S(2)}, u32[]{:S(2)}) collective-permute-start(bf16[1,768]{0,1:T(8,128)(2,1)S(1)} %get-tuple-element.49), channel_id=1, source_target_pairs={{0,8},{8,16},{16,24},{24,32},{32,40},{40,48},{48,56},{56,64},{64,7... | collective-permute-start | bytes 4616 | tf_op jit(solution)/shard_map/ppermute | solution.py:50
  122.2 7.6 %collective-permute-start.1 = (bf16[1,768]{0,1:T(8,128)(2,1)S(1)}, bf16[1,768]{0,1:T(8,128)(2,1)S(1)}, u32[]{:S(2)}, u32[]{:S(2)}) collective-permute-start(bf16[1,768]{0,1:T(8,128)(2,1)S(1)} %get-tuple-element.50), channel_id=1, source_target_pairs={{8,0},{16,8},{24,16},{32,24},{40,32},{48,40},{56,48},{64,56},{72,6... | collective-permute-start | bytes 4616 | tf_op jit(solution)/shard_map/ppermute | solution.py:51
  139.0 89.2 %all-to-all-start.2 = ((bf16[64,8,656]{2,1,0:T(8,128)(2,1)}), bf16[64,8,656]{2,1,0:T(8,128)(2,1)S(1)}, u32[]{:S(2)}, u32[]{:S(2)}) async-start(bf16[64,8,656]{2,1,0:T(8,128)(2,1)} %broadcast_in_dim.26), calls=%async_computation.2 | async-start | bytes 1572864 | tf_op jit(solution)/shard_map/all_to_all | solution.py:27
  149.5 106.8 %all-gather.14.cloned.1.call-start = ((), (), s32[]{:S(2)}) async-start(), calls=%async_computation.8 | async-start | bytes 1179648 | tf_op jit(solution)/shard_map/all_gather | solution.py:68
  174.0 58.3 %copy-start.31 = (f32[8]{0:T(128)}, f32[8]{0:T(128)S(1)}, u32[]{:S(2)}) copy-start(f32[8]{0:T(128)S(1)} %get-tuple-element.104) | copy-start | bytes 100
  174.0 58.3 %copy-start.32 = (f32[8]{0:T(128)}, f32[8]{0:T(128)S(1)}, u32[]{:S(2)}) copy-start(f32[8]{0:T(128)S(1)} %get-tuple-element.105) | copy-start | bytes 100
  174.0 58.3 %copy-start.33 = (f32[8]{0:T(128)}, f32[8]{0:T(128)S(1)}, u32[]{:S(2)}) copy-start(f32[8]{0:T(128)S(1)} %get-tuple-element.106) | copy-start | bytes 100
  174.0 58.3 %copy-start.34 = (f32[8]{0:T(128)}, f32[8]{0:T(128)S(1)}, u32[]{:S(2)}) copy-start(f32[8]{0:T(128)S(1)} %get-tuple-element.107) | copy-start | bytes 100
  174.0 58.3 %copy-start.35 = (f32[8]{0:T(128)}, f32[8]{0:T(128)S(1)}, u32[]{:S(2)}) copy-start(f32[8]{0:T(128)S(1)} %get-tuple-element.108) | copy-start | bytes 100
  228.3 109.9 %all-to-all-start.3 = ((bf16[2,256,2048]{2,1,0:T(8,128)(2,1)}), bf16[2,256,2048]{2,1,0:T(8,128)(2,1)S(1)}, u32[]{:S(2)}, u32[]{:S(2)}) async-start(bf16[2,256,2048]{2,1,0:T(8,128)(2,1)} %pad_maximum_fusion), calls=%async_computation.3 | async-start | bytes 4194304 | tf_op jit(solution)/shard_map/all_to_all | solution.py:225
  232.1 58.4 %all-gather.12.cloned.1.call-start = ((), (), s32[]{:S(2)}) async-start(), calls=%async_computation.7 | async-start | bytes 1179648 | tf_op jit(solution)/shard_map/all_gather | solution.py:68
  234.7 97.7 %all-gather.10.cloned.1.call-start = ((), (), s32[]{:S(2)}) async-start(), calls=%async_computation.6 | async-start | bytes 1179648 | tf_op jit(solution)/shard_map/all_gather | solution.py:68
  (33 other events, 410.2 us)
Sparse Core Ops, SparseCore 0:
  13.3 28.6 all-gather.7
  132.9 42.1 all-gather.15
  209.5 37.9 all-gather.13
  249.5 40.9 all-gather.11
  292.4 39.9 all-gather.9
